TPU v7x, 32 devices: a whole 2x2x4 slice. The times are simulated.
32 devices in a mesh: sp: 8 (over z, y), dp: 4 (over x, core).
Axes of the slice: x: 2, y: 2, z: 4, core: 2. Of those that a mesh axis runs over, the one named last changes fastest.
Arguments:
- query_weight: bfloat16 [4, 3072, 1024], P('dp', 'sp'), may hold values from -6 to 6
- forget_preactivation: bfloat16 [4, 3072, 1024], P('dp', 'sp'), may hold values from -7 to 7
- written_input: bfloat16 [4, 3072, 1024], P('dp', 'sp'), may hold values from -6 to 6
- output_gate_logit: bfloat16 [4, 3072, 1024], P('dp', 'sp'), may hold values from -6 to 6
- forget_floor: float32 [1024], replicated, may hold values from 0.9 to 1
- extra_log_decay: float32 [4, 3072, 16], P('dp'), may hold values from -0.7 to 0
- residual: bfloat16 [4, 3072, 2048], P('dp', 'sp'), may hold values from -6 to 6
- output_weight: bfloat16 [1024, 2048], P('dp'), may hold values from -0.1875 to 0.1875
- norm_scale_vector: float32 [2048], replicated, may hold values from 0.1 to 1.9
- expert_gate_weight: bfloat16 [8, 2048, 1024], P('sp'), may hold values from -0.125 to 0.125
- expert_up_weight: bfloat16 [8, 2048, 1024], P('sp'), may hold values from -0.125 to 0.125
- expert_down_weight: bfloat16 [8, 1024, 2048], P('sp'), may hold values from -0.1875 to 0.1875
- routes: int32 [4, 3072, 2], P('dp', 'sp'), may hold values from 0 to 7, as said below
- routing_weight: float32 [4, 3072, 2], P('dp', 'sp'), may hold values from 0.2 to 1
Outputs:
- layer_out: bfloat16 [4, 3072, 2048], P('dp', 'sp')
Inputs may be any that keep to these rules, and one draw needn't show every extreme that they name: `routes`: the two experts of a position differ and lie in one group of four, 4 g to 4 g + 3. In the positions of one device no expert is named more than 192 times. In every draw one expert is named exactly 192 times by the positions of every device, and on some devices each of the four experts of one group is named exactly 192 times.
All inputs are finite; a program needn't handle non-finite values.
Results may differ from a plain program's by a relative error of at most 0.0059.
Values may be sent and summed in bfloat16 or wider, within the bound.
A program may use at most 128 MiB of HBM per device.

v0:
```python
import functools

import jax
import jax.numpy as jnp
from jax import lax
from jax.experimental import pallas as pl
from jax.experimental.pallas import tpu as pltpu
from jax.sharding import PartitionSpec as P


HEAD_CHANNELS = 64
BLOCK = 64
PAIR = 2 * HEAD_CHANNELS
STATE_ROWS = 80
GROUP = 4
HIGHEST = lax.Precision.HIGHEST


def iota(shape, axis):
    return lax.broadcasted_iota(jnp.int32, shape, axis)


def dot_bf16(a, b, dims=((1,), (0,))):
    return lax.dot_general(
        a.astype(jnp.bfloat16),
        b.astype(jnp.bfloat16),
        (dims, ((), ())),
        preferred_element_type=jnp.float32,
    )


def three_parts(value):
    high = value.astype(jnp.bfloat16)
    rest = value - high.astype(jnp.float32)
    middle = rest.astype(jnp.bfloat16)
    low = (rest - middle.astype(jnp.float32)).astype(jnp.bfloat16)
    return high, middle, low


def mixer_kernel(
    devices,
    q_ref,
    f_ref,
    v_ref,
    gate_ref,
    floor_ref,
    extra_ref,
    out_ref,
    local_ref,
    decayed_ref,
    send_ref,
    recv_ref,
    earlier_ref,
    earlier_log_ref,
    upto_ref,
    upto_log_ref,
    send_sem,
    recv_sem,
):
    rows = q_ref.shape[1]
    pairs = local_ref.shape[0]
    rounds = send_ref.shape[0]
    heads = extra_ref.shape[1] // 3
    step = pl.program_id(0)
    place = lax.axis_index("sp")
    first = iota((1, PAIR), 1) < HEAD_CHANNELS

    def copy(number, pair):
        return pltpu.make_async_remote_copy(
            src_ref=send_ref.at[number, pair],
            dst_ref=recv_ref.at[number, pair],
            send_sem=send_sem.at[number, pair],
            recv_sem=recv_sem.at[number, pair],
            device_id={"sp": lax.rem(place + 2**number, devices)},
            device_id_type=pl.DeviceIdType.MESH,
        )

    def pack(number, pair, state, total):
        high, middle, low = three_parts(total)
        row = iota((STATE_ROWS - HEAD_CHANNELS, PAIR), 0)
        logs = jnp.where(
            row == 0,
            high.astype(jnp.float32),
            jnp.where(
                row == 1,
                middle.astype(jnp.float32),
                jnp.where(row == 2, low.astype(jnp.float32), 0.0),
            ),
        )
        send_ref[number, pair] = jnp.concatenate([state, logs], axis=0).astype(jnp.bfloat16)

    @pl.when(step == 0)
    def _():
        barrier = pltpu.get_barrier_semaphore()
        for number in range(rounds):
            for other in (place + 2**number, place + devices - 2**number):
                pl.semaphore_signal(
                    barrier,
                    inc=1,
                    device_id={"sp": lax.rem(other, devices)},
                    device_id_type=pl.DeviceIdType.MESH,
                )
        pl.semaphore_wait(barrier, 2 * rounds)

    @pl.when(step < pairs)
    def _():
        pair = step
        blocks = rows // BLOCK
        spread = (
            iota((3 * heads, PAIR), 0) % heads
            == 2 * pair + iota((3 * heads, PAIR), 1) // HEAD_CHANNELS
        ).astype(jnp.float32)
        extra = dot_bf16(extra_ref[...], spread)
        same_head = (
            iota((PAIR, PAIR), 0) // HEAD_CHANNELS == iota((PAIR, PAIR), 1) // HEAD_CHANNELS
        )
        lower = (iota((BLOCK, 3 * BLOCK), 0) >= iota((BLOCK, 3 * BLOCK), 1) % BLOCK).astype(
            jnp.float32
        )
        causal = iota((2 * BLOCK, BLOCK), 0) % BLOCK >= iota((2 * BLOCK, BLOCK), 1)
        open_share = 1.0 - floor_ref[...]
        keys = []
        logs = []
        for block in range(blocks):
            at = slice(block * BLOCK, (block + 1) * BLOCK)
            k = open_share / (1.0 + jnp.exp(f_ref[0, at, :].astype(jnp.float32)))
            keys.append(k)
            logs.append(
                jnp.concatenate(three_parts(jnp.log1p(-k) + extra[at]), axis=0)
            )
        sums = dot_bf16(lower, jnp.concatenate(logs, axis=1))
        state = jnp.zeros((PAIR, PAIR), jnp.float32)
        before = jnp.zeros((1, PAIR), jnp.float32)
        for block in range(blocks):
            at = slice(block * BLOCK, (block + 1) * BLOCK)
            q = q_ref[0, at, :].astype(jnp.float32)
            v = v_ref[0, at, :]
            k = keys[block]
            q = q / (1.0 + jnp.exp(-q))
            cumulative = sums[:, block * PAIR : (block + 1) * PAIR]
            closing = cumulative[BLOCK - 1 :, :]
            q_decayed = q * jnp.exp(cumulative)
            k_grown = k * jnp.exp(-cumulative)
            k_closing = k * jnp.exp(closing - cumulative)
            stacked = jnp.concatenate(
                [jnp.where(first, q_decayed, 0.0), jnp.where(first, 0.0, q_decayed)], axis=0
            )
            scores = jnp.where(causal, dot_bf16(stacked, k_grown, ((1,), (1,))), 0.0)
            inner = dot_bf16(scores, v)
            inner = jnp.where(first, inner[:BLOCK], inner[BLOCK:])
            local_ref[pair, at, :] = inner + dot_bf16(q_decayed, state, ((1,), (1,)))
            decayed_ref[pair, at, :] = (q_decayed * jnp.exp(before)).astype(jnp.bfloat16)
            state = state * jnp.exp(closing) + jnp.where(
                same_head, dot_bf16(v, k_closing, ((0,), (0,))), 0.0
            )
            before = before + closing
        folded = jnp.where(first, state[:HEAD_CHANNELS], state[HEAD_CHANNELS:])
        upto_ref[pair] = folded
        upto_log_ref[pair] = jnp.broadcast_to(before, (8, PAIR))
        earlier_ref[pair] = jnp.zeros((HEAD_CHANNELS, PAIR), jnp.float32)
        earlier_log_ref[pair] = jnp.zeros((8, PAIR), jnp.float32)

        @pl.when(place + 1 < devices)
        def _():
            pack(0, pair, folded, before)
            copy(0, pair).start()

    def merge(number):
        distance = 2**number
        pair = step - 1 - number

        @pl.when((pair >= 0) & (pair < pairs))
        def _():
            @pl.when(place >= distance)
            def _():
                copy(number, pair).wait_recv()
                item = recv_ref[number, pair].astype(jnp.float32)
                state = item[:HEAD_CHANNELS]
                total = jnp.sum(item[HEAD_CHANNELS:], axis=0, keepdims=True)
                log = earlier_log_ref[pair][:1]
                earlier_ref[pair] = state * jnp.exp(log) + earlier_ref[pair]
                earlier_log_ref[pair] = jnp.broadcast_to(log + total, (8, PAIR))
                if number + 1 < rounds:
                    log = upto_log_ref[pair][:1]
                    upto_ref[pair] = state * jnp.exp(log) + upto_ref[pair]
                    upto_log_ref[pair] = jnp.broadcast_to(log + total, (8, PAIR))

            if number + 1 < rounds:

                @pl.when(place + 2 * distance < devices)
                def _():
                    pack(number + 1, pair, upto_ref[pair], upto_log_ref[pair][:1])
                    copy(number + 1, pair).start()

    for number in range(rounds):
        merge(number)

    pair = step - rounds

    @pl.when(pair >= 0)
    def _():
        state = earlier_ref[pair]
        state = jnp.concatenate(
            [jnp.where(first, state, 0.0), jnp.where(first, 0.0, state)], axis=0
        )
        value = local_ref[pair] + dot_bf16(decayed_ref[pair], state, ((1,), (1,)))
        same_head = (
            iota((2 * PAIR, PAIR), 0) // HEAD_CHANNELS % 2 == iota((2 * PAIR, PAIR), 1) // HEAD_CHANNELS
        ).astype(jnp.float32)
        square = value * value
        high = square.astype(jnp.bfloat16)
        low = (square - high.astype(jnp.float32)).astype(jnp.bfloat16)
        mean = dot_bf16(jnp.concatenate([high, low], axis=1), same_head) * (1.0 / HEAD_CHANNELS)
        gate = gate_ref[0].astype(jnp.float32)
        gate = gate / (1.0 + jnp.exp(-gate))
        out_ref[...] = (value * lax.rsqrt(mean + 1e-06) * gate).astype(jnp.bfloat16)

    @pl.when(step == pairs + rounds - 1)
    def _():
        for number in range(rounds):

            @pl.when(place + 2**number < devices)
            def _():
                for pair in range(pairs):
                    copy(number, pair).wait_send()


def mixer(query, forget, value, gate, floor, extra, devices):
    rows, width = query.shape[1:]
    pairs = width // PAIR
    rounds = (devices - 1).bit_length()
    early = pl.BlockSpec((1, rows, PAIR), lambda s: (0, 0, jnp.minimum(s, pairs - 1)))
    late = pl.BlockSpec((1, rows, PAIR), lambda s: (0, 0, jnp.maximum(s - rounds, 0)))
    return pl.pallas_call(
        functools.partial(mixer_kernel, devices),
        grid=(pairs + rounds,),
        in_specs=[
            early,
            early,
            early,
            late,
            pl.BlockSpec((1, PAIR), lambda s: (0, jnp.minimum(s, pairs - 1))),
            pl.BlockSpec((rows, extra.shape[1] * 3), lambda s: (0, 0)),
        ],
        out_specs=pl.BlockSpec((rows, PAIR), lambda s: (0, jnp.maximum(s - rounds, 0))),
        out_shape=jax.ShapeDtypeStruct((rows, width), jnp.bfloat16),
        scratch_shapes=[
            pltpu.VMEM((pairs, rows, PAIR), jnp.float32),
            pltpu.VMEM((pairs, rows, PAIR), jnp.bfloat16),
            pltpu.VMEM((rounds, pairs, STATE_ROWS, PAIR), jnp.bfloat16),
            pltpu.VMEM((rounds, pairs, STATE_ROWS, PAIR), jnp.bfloat16),
            pltpu.VMEM((pairs, HEAD_CHANNELS, PAIR), jnp.float32),
            pltpu.VMEM((pairs, 8, PAIR), jnp.float32),
            pltpu.VMEM((pairs, HEAD_CHANNELS, PAIR), jnp.float32),
            pltpu.VMEM((pairs, 8, PAIR), jnp.float32),
            pltpu.SemaphoreType.DMA((rounds, pairs)),
            pltpu.SemaphoreType.DMA((rounds, pairs)),
        ],
        compiler_params=pltpu.CompilerParams(collective_id=0, has_side_effects=True),
        cost_estimate=pl.CostEstimate(
            flops=rows * width * 2 * 64 * 50, bytes_accessed=rows * width * 10, transcendentals=0
        ),
    )(
        query,
        forget,
        value,
        gate,
        floor.reshape(1, width),
        jnp.concatenate(three_parts(extra), axis=1),
    )


def positions_of(hit):
    rows = hit.shape[0]
    lower = (iota((rows, rows), 0) >= iota((rows, rows), 1)).astype(jnp.bfloat16)
    count = jnp.dot(lower, hit.astype(jnp.bfloat16), preferred_element_type=jnp.float32)
    return jnp.where(hit, count - 1.0, -1.0)


def spread_kinds(values, width):
    kinds = values.shape[1]
    wide = (iota((kinds, kinds * width), 1) // width == iota((kinds, kinds * width), 0)).astype(
        jnp.bfloat16
    )
    return jnp.dot(values.astype(jnp.bfloat16), wide, preferred_element_type=jnp.float32)


def pick_rows(chosen, rows):
    return lax.dot_general(
        chosen.astype(jnp.bfloat16),
        rows,
        (((0,), (0,)), ((), ())),
        preferred_element_type=jnp.float32,
    ).astype(jnp.bfloat16)


def weigh_rows(weights, rows):
    high, low = weights
    return jnp.dot(high, rows, preferred_element_type=jnp.float32) + jnp.dot(
        low, rows, preferred_element_type=jnp.float32
    )


def per_device(
    query_weight,
    forget_preactivation,
    written_input,
    output_gate_logit,
    forget_floor,
    extra_log_decay,
    residual,
    output_weight,
    norm_scale_vector,
    expert_gate_weight,
    expert_up_weight,
    expert_down_weight,
    routes,
    routing_weight,
):
    seq_count, tok_rows, mix_width = query_weight.shape
    model_width = output_weight.shape[1]
    place = lax.axis_index("sp")
    devices = lax.axis_size("sp")
    groups = devices // GROUP
    capacity = 4 * tok_rows // devices
    group_capacity = 2 * capacity
    my_group, my_local = place // GROUP, place % GROUP

    copies = lax.axis_size("dp")
    my_copy = lax.axis_index("dp")

    picks = routes.reshape(tok_rows, 2)
    weights = routing_weight.reshape(tok_rows, 2)
    relative = (picks[:, :1] // GROUP - my_group + groups) % groups
    own_local = jnp.where(relative == 0, picks % GROUP, -1)
    peers = jnp.arange(GROUP, dtype=jnp.int32) ^ my_local

    def plan(local):
        first = local[:, :1] == peers
        second = local[:, 1:] == peers
        position = positions_of(first | second)
        rows, kinds = position.shape
        slot = (iota((rows, kinds * capacity), 1) % capacity).astype(jnp.float32)
        chosen = spread_kinds(position, capacity) == slot
        return lax.optimization_barrier(chosen.astype(jnp.bfloat16))

    def weigh_tables(local, share, chosen):
        weight = jnp.where(local[:, :1] == peers, share[:, :1], 0.0) + jnp.where(
            local[:, 1:] == peers, share[:, 1:], 0.0
        )
        high = weight.astype(jnp.bfloat16)
        low = (weight - high.astype(jnp.float32)).astype(jnp.bfloat16)
        return lax.optimization_barrier(
            tuple(
                (spread_kinds(half, capacity) * chosen.astype(jnp.float32)).astype(jnp.bfloat16)
                for half in (high, low)
            )
        )

    own_plan = plan(own_local)
    leaves = positions_of(relative == jnp.arange(1, groups, dtype=jnp.int32)[None, :])
    place_in_group = iota((tok_rows, group_capacity), 1).astype(jnp.float32)
    crossing = jnp.concatenate(
        [leaves[:, number : number + 1] == place_in_group for number in range(groups - 1)], axis=1
    )
    notes = jnp.concatenate([(picks % GROUP + 1).astype(jnp.float32), weights], axis=1)
    noted = lax.dot_general(
        crossing.astype(jnp.float32), notes, (((0,), (0,)), ((), ())), precision=HIGHEST
    )

    def hop(array, distance):
        pairs = [(d, (d + GROUP * distance) % devices) for d in range(devices)]
        return lax.ppermute(array, "sp", pairs)

    def part(array, number, size):
        return lax.slice_in_dim(array, number * size, (number + 1) * size, axis=0)

    told = [
        hop(part(noted, distance - 1, group_capacity), distance)
        for distance in range(1, groups)
    ]

    extra = lax.dynamic_slice_in_dim(extra_log_decay[0], place * tok_rows, tok_rows, 0)
    mixer_out = mixer(
        query_weight,
        forget_preactivation,
        written_input,
        output_gate_logit,
        forget_floor,
        extra,
        devices,
    )

    shares = output_weight
    step = copies // 2
    order = [0]
    while step:
        other = lax.ppermute(shares, "dp", [(d, d ^ step) for d in range(copies)])
        if step == copies // 2:
            other, mixer_out = lax.optimization_barrier((other, mixer_out))
        shares = jnp.concatenate([shares, other], axis=0)
        order = order + [held ^ step for held in order]
        step //= 2

    share_width = mix_width // copies
    mixer_out = jnp.concatenate(
        [
            lax.dynamic_slice_in_dim(mixer_out, (my_copy ^ held) * share_width, share_width, 1)
            for held in order
        ],
        axis=1,
    )
    projected = jnp.dot(mixer_out, shares, preferred_element_type=jnp.float32)
    updated = (residual.reshape(tok_rows, model_width).astype(jnp.float32) + projected).astype(
        jnp.bfloat16
    )
    widened = updated.astype(jnp.float32)
    normed = (
        widened
        * lax.rsqrt(jnp.mean(widened * widened, axis=-1, keepdims=True) + 1e-06)
        * norm_scale_vector
    ).astype(jnp.bfloat16)

    def experts(rows):
        gate = jnp.dot(rows, expert_gate_weight[0], preferred_element_type=jnp.float32)
        up = jnp.dot(rows, expert_up_weight[0], preferred_element_type=jnp.float32)
        hidden = (jax.nn.silu(gate) * up).astype(jnp.bfloat16)
        return jnp.dot(
            hidden, expert_down_weight[0], preferred_element_type=jnp.float32
        ).astype(jnp.bfloat16)

    def swapped(blocks):
        moved = {
            bits: lax.ppermute(blocks[bits], "sp", [(d, d ^ bits) for d in range(devices)])
            for bits in range(GROUP - 1, 0, -1)
        }
        return [blocks[0]] + [moved[bits] for bits in range(1, GROUP)]

    def blocks_of(array):
        return [part(array, bits, capacity) for bits in range(GROUP)]

    leaving = pick_rows(crossing, normed)
    arrived = [
        hop(part(leaving, distance - 1, group_capacity), distance)
        for distance in range(1, groups)
    ]
    own_rows = pick_rows(own_plan, normed)
    late = (weights, own_plan, *told, own_rows)
    weights, own_plan, *told, own_rows = lax.optimization_barrier(late)
    own = swapped(blocks_of(own_rows))
    locals_told = [jnp.round(t[:, :2]).astype(jnp.int32) - 1 for t in told]
    plans = [plan(local) for local in locals_told]
    tables = [weigh_tables(own_local, weights, own_plan)] + [
        weigh_tables(local, t[:, 2:], chosen)
        for local, t, chosen in zip(locals_told, told, plans)
    ]
    given = [swapped(blocks_of(pick_rows(p, rows))) for p, rows in zip(plans, arrived)]
    own_made = experts(jnp.concatenate(own, axis=0))
    back = []
    for number, blocks in enumerate(given, 1):
        made = experts(jnp.concatenate(blocks, axis=0))
        made = swapped(blocks_of(made))
        total = weigh_rows(tables[number], jnp.concatenate(made, axis=0)).astype(jnp.bfloat16)
        back.append(hop(total, groups - number))
    own_made = jnp.concatenate(swapped(blocks_of(own_made)), axis=0)
    summed = weigh_rows(tables[0], own_made)
    if back:
        summed = summed + jnp.dot(
            crossing.astype(jnp.bfloat16),
            jnp.concatenate(back, axis=0),
            preferred_element_type=jnp.float32,
        )
    layer_out = (widened + summed).astype(jnp.bfloat16)
    return layer_out.reshape(seq_count, tok_rows, model_width)


def solution(mesh):
    placed = (
        P("dp", "sp", None),
        P("dp", "sp", None),
        P("dp", "sp", None),
        P("dp", "sp", None),
        P(),
        P("dp", None, None),
        P("dp", "sp", None),
        P("dp", None),
        P(),
        P("sp", None, None),
        P("sp", None, None),
        P("sp", None, None),
        P("dp", "sp", None),
        P("dp", "sp", None),
    )

    return jax.shard_map(
        per_device, mesh=mesh, in_specs=placed, out_specs=P("dp", "sp", None), check_vma=False
    )
```

profile of v0, /device:TPU:0, one launch (start us, length us, event | category | flops | bytes accessed | tf_op | source)
XLA Modules:
  0.0 291.6 jit_solution(8052365545905675966)
XLA Ops:
  0.0 3.0 %collective-permute-start = (bf16[256,2048]{1,0:T(8,128)(2,1)}, bf16[256,2048]{1,0:T(8,128)(2,1)}, u32[]{:S(2)}, u32[]{:S(2)}) collective-permute-start(bf16[256,2048]{1,0:T(8,128)(2,1)} %param.21), channel_id=1, source_target_pairs={{0,2},{1,3},{2,0},{3,1},{4,6},{5,7},{6,4},{7,5},{8,10},{9,11},{10,... | collective-permute-start | bytes 3145736 | tf_op jit(solution)/shard_map/ppermute | solution.py:398
  5.5 22.3 %shard_map.136 = bf16[384,1024]{1,0:T(8,128)(2,1)} custom-call(bf16[1,384,1024]{2,1,0:T(8,128)(2,1)} %q_ref.1, bf16[1,384,1024]{2,1,0:T(8,128)(2,1)} %f_ref.1, bf16[1,384,1024]{2,1,0:T(8,128)(2,1)} %v_ref.1, bf16[1,384,1024]{2,1,0:T(8,128)(2,1)} %gate_ref.1, f32[1,1024]{1,0:T(1,128)} %bitcast.55, bf16[384,48]{1,0:T(8,128)(2,1)} %copy.16.extra_ref), custom_call_target="tpu_custom_call" | custom-call | flops 2516582400 | bytes 3932160 | tf_op jit(solution)/shard_map/pallas_call | solution.py:234
  30.2 8.6 %collective-permute-start.2 = (f32[384,4]{0,1:T(4,128)S(1)}, f32[384,4]{0,1:T(4,128)S(1)}, u32[]{:S(2)}, u32[]{:S(2)}) collective-permute-start(f32[384,4]{0,1:T(4,128)S(1)} %fusion.47), channel_id=1, source_target_pairs={{0,16},{4,20},{8,24},{12,28},{16,0},{20,4},{24,8},{28,12},{1,17},{... | collective-permute-start | bytes 18440 | tf_op jit(solution)/shard_map/ppermute | solution.py:373
  39.8 4.7 %fusion.24 = (f32[384]{0:T(512)S(1)}, bf16[384,2048]{1,0:T(8,128)(2,1)S(1)}) fusion(bf16[512,2048]{1,0:T(8,128)(2,1)} %collective-permute-done.1, bf16[256,2048]{1,0:T(8,128)(2,1)} %collective-permute-done, bf16[256,2048]{1,0:T(8,128)(2,1)} %param.21, bf16[384,256]{1,0:T(8,128)(2,1)S(1)} %get-tuple-element.57, bf16[384,256]{1,0:T(8,128)(2,1)S(1)} %get-tuple-element.58, ...), kind=kOutput, calls=%fused_computation.25 | convolution fusion | flops 1631059584 | bytes 8128000 | tf_op jit(solution)/shard_map/dot_general | solution.py:413
  49.4 2.8 collective-permute-start.9
  62.6 10.7 %collective-permute-done.3 = bf16[192,2048]{1,0:T(8,128)(2,1)} collective-permute-done((bf16[192,2048]{1,0:T(8,128)(2,1)}, bf16[192,2048]{1,0:T(8,128)(2,1)}, u32[]{:S(2)}, u32[]{:S(2)}) %collective-permute-start.3) | collective-permute-done | bytes 786464 | tf_op jit(solution)/shard_map/ppermute | solution.py:434
  73.3 31.0 %collective-permute-done.4 = bf16[192,2048]{1,0:T(8,128)(2,1)} collective-permute-done((bf16[192,2048]{1,0:T(8,128)(2,1)}, bf16[192,2048]{1,0:T(8,128)(2,1)}, u32[]{:S(2)}, u32[]{:S(2)}) %collective-permute-start.4) | collective-permute-done | bytes 786464 | tf_op jit(solution)/shard_map/ppermute | solution.py:434
  104.2 20.0 %collective-permute-done.5 = bf16[192,2048]{1,0:T(8,128)(2,1)} collective-permute-done((bf16[192,2048]{1,0:T(8,128)(2,1)}, bf16[192,2048]{1,0:T(8,128)(2,1)}, u32[]{:S(2)}, u32[]{:S(2)}) %collective-permute-start.5) | collective-permute-done | bytes 786464 | tf_op jit(solution)/shard_map/ppermute | solution.py:434
  124.2 7.3 %fusion.16 = f32[768,1024]{1,0:T(8,128)S(1)} fusion(bf16[1,2048,1024]{2,1,0:T(8,128)(2,1)} %param.23, bf16[192,2048]{1,0:T(8,128)(2,1)} %collective-permute-done.5, bf16[192,2048]{1,0:T(8,128)(2,1)} %collective-permute-done.4, bf16[192,2048]{1,0:T(8,128)(2,1)} %collective-permute-done.3, bf16[192,2048]{1,0:T(8,128)(2,1)S(1)} %get-tuple-element.52), kind=kOutput, calls=%fused_computation.19 | convolution fusion | flops 3233808384 | bytes 10485760 | tf_op jit(solution)/shard_map/dot_general | solution.py:425
  131.5 3.2 %convolution_convert_fusion = bf16[768,2048]{1,0:T(8,128)(2,1)S(1)} fusion(bf16[384,768]{1,0:T(8,128)(2,1)S(1)} %fusion.39, bf16[384,2048]{1,0:T(8,128)(2,1)} %collective-permute-done.9), kind=kOutput, calls=%fused_computation.23 | convolution fusion | flops 1209532416 | bytes 5308416 | tf_op jit(solution)/shard_map/dot_general | solution.py:289
  135.3 3.3 %collective-permute-start.12 = (bf16[192,2048]{1,0:T(8,128)(2,1)S(1)}, bf16[192,2048]{1,0:T(8,128)(2,1)S(1)}, u32[]{:S(2)}, u32[]{:S(2)}) collective-permute-start(bf16[192,2048]{1,0:T(8,128)(2,1)S(1)} %get-tuple-element.45), channel_id=1, source_target_pairs={{0,12},{4,8},{8,4},{12,0},{16,28},{20,24},{24,20},{28,16},{1,13},{... | collective-permute-start | bytes 2359304 | tf_op jit(solution)/shard_map/ppermute | solution.py:434
  138.6 5.8 %fusion.12 = f32[768,1024]{1,0:T(8,128)S(1)} fusion(bf16[1,2048,1024]{2,1,0:T(8,128)(2,1)S(1)} %copy-done.14, bf16[192,2048]{1,0:T(8,128)(2,1)} %collective-permute-done.5, bf16[192,2048]{1,0:T(8,128)(2,1)} %collective-permute-done.4, bf16[192,2048]{1,0:T(8,128)(2,1)} %collective-permute-done.3, bf16[192,2048]{1,0:T(8,128)(2,1)S(1)} %get-tuple-element.52), kind=kOutput, calls=%fused_computation.15 | convolution fusion | flops 3233808384 | bytes 10485760 | tf_op jit(solution)/shard_map/dot_general | solution.py:426
  144.4 10.2 %collective-permute-done.10 = bf16[192,2048]{1,0:T(8,128)(2,1)S(1)} collective-permute-done((bf16[192,2048]{1,0:T(8,128)(2,1)S(1)}, bf16[192,2048]{1,0:T(8,128)(2,1)S(1)}, u32[]{:S(2)}, u32[]{:S(2)}) %collective-permute-start.10) | collective-permute-done | bytes 786464 | tf_op jit(solution)/shard_map/ppermute | solution.py:434
  155.7 15.9 %collective-permute-done.12 = bf16[192,2048]{1,0:T(8,128)(2,1)S(1)} collective-permute-done((bf16[192,2048]{1,0:T(8,128)(2,1)S(1)}, bf16[192,2048]{1,0:T(8,128)(2,1)S(1)}, u32[]{:S(2)}, u32[]{:S(2)}) %collective-permute-start.12) | collective-permute-done | bytes 786464 | tf_op jit(solution)/shard_map/ppermute | solution.py:434
  171.6 3.4 %fusion.14 = f32[768,1024]{1,0:T(8,128)S(1)} fusion(bf16[1,2048,1024]{2,1,0:T(8,128)(2,1)S(1)} %copy-done.13, bf16[192,2048]{1,0:T(8,128)(2,1)S(1)} %collective-permute-done.12, bf16[192,2048]{1,0:T(8,128)(2,1)S(1)} %collective-permute-done.11, bf16[192,2048]{1,0:T(8,128)(2,1)S(1)} %collective-permute-done.10, bf16[192,2048]{1,0:T(8,128)(2,1)S(1)} %get-tuple-element.44), kind=kOutput, calls=%fused_computation.17 | convolution fusion | flops 3233808384 | bytes 10485760 | tf_op jit(solution)/shard_map/dot_general | solution.py:425
  175.0 3.4 %fusion.10 = f32[768,1024]{1,0:T(8,128)S(1)} fusion(bf16[1,2048,1024]{2,1,0:T(8,128)(2,1)S(1)} %copy-done.14, bf16[192,2048]{1,0:T(8,128)(2,1)S(1)} %collective-permute-done.12, bf16[192,2048]{1,0:T(8,128)(2,1)S(1)} %collective-permute-done.11, bf16[192,2048]{1,0:T(8,128)(2,1)S(1)} %collective-permute-done.10, bf16[192,2048]{1,0:T(8,128)(2,1)S(1)} %get-tuple-element.44), kind=kOutput, calls=%fused_computation.13 | convolution fusion | flops 3233808384 | bytes 10485760 | tf_op jit(solution)/shard_map/dot_general | solution.py:426
  178.5 3.8 %fusion.21 = bf16[768,2048]{1,0:T(8,128)(2,1)S(1)} fusion(bf16[1,1024,2048]{2,1,0:T(8,128)(2,1)S(1)} %copy-done.15, f32[768,1024]{1,0:T(8,128)S(1)} %fusion.10, f32[768,1024]{1,0:T(8,128)S(1)} %fusion.14), kind=kOutput, calls=%fused_computation.22 | convolution fusion | flops 3227516928 | bytes 13631488 | tf_op jit(solution)/shard_map/dot_general | solution.py:428
  183.4 2.8 collective-permute-start.15
  186.2 4.0 %fusion.18 = bf16[768,2048]{1,0:T(8,128)(2,1)S(1)} fusion(bf16[1,1024,2048]{2,1,0:T(8,128)(2,1)S(1)} %copy-done.15, f32[768,1024]{1,0:T(8,128)S(1)} %fusion.12, f32[768,1024]{1,0:T(8,128)S(1)} %fusion.16), kind=kOutput, calls=%fused_computation.21 | convolution fusion | flops 3227516928 | bytes 13631488 | tf_op jit(solution)/shard_map/dot_general | solution.py:428
  191.3 27.2 %collective-permute-done.13 = bf16[192,2048]{1,0:T(8,128)(2,1)S(1)} collective-permute-done((bf16[192,2048]{1,0:T(8,128)(2,1)S(1)}, bf16[192,2048]{1,0:T(8,128)(2,1)S(1)}, u32[]{:S(2)}, u32[]{:S(2)}) %collective-permute-start.13) | collective-permute-done | bytes 786464 | tf_op jit(solution)/shard_map/ppermute | solution.py:434
  218.6 2.9 %collective-permute-done.15 = bf16[192,2048]{1,0:T(8,128)(2,1)S(1)} collective-permute-done((bf16[192,2048]{1,0:T(8,128)(2,1)S(1)}, bf16[192,2048]{1,0:T(8,128)(2,1)S(1)}, u32[]{:S(2)}, u32[]{:S(2)}) %collective-permute-start.15) | collective-permute-done | bytes 786464 | tf_op jit(solution)/shard_map/ppermute | solution.py:434
  227.9 5.9 %collective-permute-done.6 = bf16[192,2048]{1,0:T(8,128)(2,1)S(1)} collective-permute-done((bf16[192,2048]{1,0:T(8,128)(2,1)S(1)}, bf16[192,2048]{1,0:T(8,128)(2,1)S(1)}, u32[]{:S(2)}, u32[]{:S(2)}) %collective-permute-start.6) | collective-permute-done | bytes 786464 | tf_op jit(solution)/shard_map/ppermute | solution.py:434
  233.8 34.5 %collective-permute-done.7 = bf16[192,2048]{1,0:T(8,128)(2,1)S(1)} collective-permute-done((bf16[192,2048]{1,0:T(8,128)(2,1)S(1)}, bf16[192,2048]{1,0:T(8,128)(2,1)S(1)}, u32[]{:S(2)}, u32[]{:S(2)}) %collective-permute-start.7) | collective-permute-done | bytes 786464 | tf_op jit(solution)/shard_map/ppermute | solution.py:434
  268.3 15.2 %collective-permute-done.8 = bf16[192,2048]{1,0:T(8,128)(2,1)S(1)} collective-permute-done((bf16[192,2048]{1,0:T(8,128)(2,1)S(1)}, bf16[192,2048]{1,0:T(8,128)(2,1)S(1)}, u32[]{:S(2)}, u32[]{:S(2)}) %collective-permute-start.8) | collective-permute-done | bytes 786464 | tf_op jit(solution)/shard_map/ppermute | solution.py:434
  (97 shorter events, 39.2 us)
Async XLA Ops:
  0.0 27.8 %collective-permute-start = (bf16[256,2048]{1,0:T(8,128)(2,1)}, bf16[256,2048]{1,0:T(8,128)(2,1)}, u32[]{:S(2)}, u32[]{:S(2)}) collective-permute-start(bf16[256,2048]{1,0:T(8,128)(2,1)} %param.21), channel_id=1, source_target_pairs={{0,2},{1,3},{2,0},{3,1},{4,6},{5,7},{6,4},{7,5},{8,10},{9,11},{10,... | collective-permute-start | bytes 3145736 | tf_op jit(solution)/shard_map/ppermute | solution.py:398
  27.8 11.9 %copy-start = (bf16[384,1024]{1,0:T(8,128)(2,1)S(1)}, bf16[384,1024]{1,0:T(8,128)(2,1)}, u32[]{:S(2)}) copy-start(bf16[384,1024]{1,0:T(8,128)(2,1)} %shard_map.136) | copy-start | bytes 2359300
  29.6 10.1 %collective-permute-start.1 = (bf16[512,2048]{1,0:T(8,128)(2,1)S(1)}, bf16[512,2048]{1,0:T(8,128)(2,1)}, u32[]{:S(2)}, u32[]{:S(2)}) collective-permute-start(bf16[512,2048]{1,0:T(8,128)(2,1)S(1)} %pad_maximum_fusion.4), channel_id=1, source_target_pairs={{0,1},{1,0},{2,3},{3,2},{4,5},{5,4},{6,7},{7,6},{8,9},{9,8},{10,11... | collective-permute-start | bytes 6291464 | tf_op jit(solution)/shard_map/ppermute | solution.py:398
  29.7 16.8 %copy-start.3 = (f32[384]{0:T(512)}, f32[384]{0:T(512)S(1)}, u32[]{:S(2)}) copy-start(f32[384]{0:T(512)S(1)} %iota_convert_fusion) | copy-start | bytes 4612
  29.8 16.8 %copy-start.5 = (f32[384]{0:T(512)}, f32[384]{0:T(512)S(1)}, u32[]{:S(2)}) copy-start(f32[384]{0:T(512)S(1)} %fusion.121) | copy-start | bytes 4612
  30.2 18.7 %collective-permute-start.2 = (f32[384,4]{0,1:T(4,128)S(1)}, f32[384,4]{0,1:T(4,128)S(1)}, u32[]{:S(2)}, u32[]{:S(2)}) collective-permute-start(f32[384,4]{0,1:T(4,128)S(1)} %fusion.47), channel_id=1, source_target_pairs={{0,16},{4,20},{8,24},{12,28},{16,0},{20,4},{24,8},{28,12},{1,17},{... | collective-permute-start | bytes 18440 | tf_op jit(solution)/shard_map/ppermute | solution.py:373
  38.8 5.7 %copy-start.1 = (s32[4]{0:T(128)}, s32[4]{0:T(128)S(1)}, u32[]{:S(2)}) copy-start(s32[4]{0:T(128)S(1)} %iota_xor_fusion) | copy-start | bytes 52
  38.8 5.7 %copy-start.17 = (pred[768]{0:T(1024)(128)(4,1)}, pred[768]{0:T(1024)(128)(4,1)S(1)}, u32[]{:S(2)}) copy-start(pred[768]{0:T(1024)(128)(4,1)S(1)} %fusion.116) | copy-start | bytes 2308
  48.8 9.2 %copy-start.8 = (f32[384,4]{0,1:T(4,128)}, f32[384,4]{0,1:T(4,128)S(1)}, u32[]{:S(2)}) copy-start(f32[384,4]{0,1:T(4,128)S(1)} %collective-permute-done.2) | copy-start | bytes 18436
  49.4 82.1 %collective-permute-start.9 = (bf16[384,2048]{1,0:T(8,128)(2,1)}, bf16[384,2048]{1,0:T(8,128)(2,1)}, u32[]{:S(2)}, u32[]{:S(2)}) collective-permute-start(bf16[384,2048]{1,0:T(8,128)(2,1)} %convolution_convert_fusion.2), channel_id=1, source_target_pairs={{0,16},{4,20},{8,24},{12,28},{16,0},{20,4},{24,8},{28,12},{1,17},{... | collective-permute-start | bytes 4718600 | tf_op jit(solution)/shard_map/ppermute | solution.py:373
  53.6 19.6 %collective-permute-start.3 = (bf16[192,2048]{1,0:T(8,128)(2,1)}, bf16[192,2048]{1,0:T(8,128)(2,1)}, u32[]{:S(2)}, u32[]{:S(2)}) collective-permute-start(bf16[192,2048]{1,0:T(8,128)(2,1)} %get-tuple-element.55), channel_id=1, source_target_pairs={{0,4},{4,0},{8,12},{12,8},{16,20},{20,16},{24,28},{28,24},{1,5},{5... | collective-permute-start | bytes 2359304 | tf_op jit(solution)/shard_map/ppermute | solution.py:434
  54.8 49.4 %collective-permute-start.4 = (bf16[192,2048]{1,0:T(8,128)(2,1)}, bf16[192,2048]{1,0:T(8,128)(2,1)}, u32[]{:S(2)}, u32[]{:S(2)}) collective-permute-start(bf16[192,2048]{1,0:T(8,128)(2,1)} %get-tuple-element.54), channel_id=1, source_target_pairs={{0,8},{4,12},{8,0},{12,4},{16,24},{20,28},{24,16},{28,20},{1,9},{5... | collective-permute-start | bytes 2359304 | tf_op jit(solution)/shard_map/ppermute | solution.py:434
  57.2 67.0 %collective-permute-start.5 = (bf16[192,2048]{1,0:T(8,128)(2,1)}, bf16[192,2048]{1,0:T(8,128)(2,1)}, u32[]{:S(2)}, u32[]{:S(2)}) collective-permute-start(bf16[192,2048]{1,0:T(8,128)(2,1)} %get-tuple-element.53), channel_id=1, source_target_pairs={{0,12},{4,8},{8,4},{12,0},{16,28},{20,24},{24,20},{28,16},{1,13},{... | collective-permute-start | bytes 2359304 | tf_op jit(solution)/shard_map/ppermute | solution.py:434
  135.0 19.6 %collective-permute-start.10 = (bf16[192,2048]{1,0:T(8,128)(2,1)S(1)}, bf16[192,2048]{1,0:T(8,128)(2,1)S(1)}, u32[]{:S(2)}, u32[]{:S(2)}) collective-permute-start(bf16[192,2048]{1,0:T(8,128)(2,1)S(1)} %get-tuple-element.47), channel_id=1, source_target_pairs={{0,4},{4,0},{8,12},{12,8},{16,20},{20,16},{24,28},{28,24},{1,5},{5... | collective-permute-start | bytes 2359304 | tf_op jit(solution)/shard_map/ppermute | solution.py:434
  135.2 20.4 %collective-permute-start.11 = (bf16[192,2048]{1,0:T(8,128)(2,1)S(1)}, bf16[192,2048]{1,0:T(8,128)(2,1)S(1)}, u32[]{:S(2)}, u32[]{:S(2)}) collective-permute-start(bf16[192,2048]{1,0:T(8,128)(2,1)S(1)} %get-tuple-element.46), channel_id=1, source_target_pairs={{0,8},{4,12},{8,0},{12,4},{16,24},{20,28},{24,16},{28,20},{1,9},{5... | collective-permute-start | bytes 2359304 | tf_op jit(solution)/shard_map/ppermute | solution.py:434
  135.3 36.3 %copy-start.13 = (bf16[1,2048,1024]{2,1,0:T(8,128)(2,1)S(1)}, bf16[1,2048,1024]{2,1,0:T(8,128)(2,1)}, u32[]{:S(2)}) copy-start(bf16[1,2048,1024]{2,1,0:T(8,128)(2,1)} %param.23) | copy-start | bytes 12582916
  135.3 36.3 %collective-permute-start.12 = (bf16[192,2048]{1,0:T(8,128)(2,1)S(1)}, bf16[192,2048]{1,0:T(8,128)(2,1)S(1)}, u32[]{:S(2)}, u32[]{:S(2)}) collective-permute-start(bf16[192,2048]{1,0:T(8,128)(2,1)S(1)} %get-tuple-element.45), channel_id=1, source_target_pairs={{0,12},{4,8},{8,4},{12,0},{16,28},{20,24},{24,20},{28,16},{1,13},{... | collective-permute-start | bytes 2359304 | tf_op jit(solution)/shard_map/ppermute | solution.py:434
  182.7 35.8 %collective-permute-start.13 = (bf16[192,2048]{1,0:T(8,128)(2,1)S(1)}, bf16[192,2048]{1,0:T(8,128)(2,1)S(1)}, u32[]{:S(2)}, u32[]{:S(2)}) collective-permute-start(bf16[192,2048]{1,0:T(8,128)(2,1)S(1)} %get-tuple-element.43), channel_id=1, source_target_pairs={{0,4},{4,0},{8,12},{12,8},{16,20},{20,16},{24,28},{28,24},{1,5},{5... | collective-permute-start | bytes 2359304 | tf_op jit(solution)/shard_map/ppermute | solution.py:434
  183.1 35.5 %collective-permute-start.14 = (bf16[192,2048]{1,0:T(8,128)(2,1)S(1)}, bf16[192,2048]{1,0:T(8,128)(2,1)S(1)}, u32[]{:S(2)}, u32[]{:S(2)}) collective-permute-start(bf16[192,2048]{1,0:T(8,128)(2,1)S(1)} %get-tuple-element.42), channel_id=1, source_target_pairs={{0,8},{4,12},{8,0},{12,4},{16,24},{20,28},{24,16},{28,20},{1,9},{5... | collective-permute-start | bytes 2359304 | tf_op jit(solution)/shard_map/ppermute | solution.py:434
  183.4 38.1 %collective-permute-start.15 = (bf16[192,2048]{1,0:T(8,128)(2,1)S(1)}, bf16[192,2048]{1,0:T(8,128)(2,1)S(1)}, u32[]{:S(2)}, u32[]{:S(2)}) collective-permute-start(bf16[192,2048]{1,0:T(8,128)(2,1)S(1)} %get-tuple-element.41), channel_id=1, source_target_pairs={{0,12},{4,8},{8,4},{12,0},{16,28},{20,24},{24,20},{28,16},{1,13},{... | collective-permute-start | bytes 2359304 | tf_op jit(solution)/shard_map/ppermute | solution.py:434
  190.6 43.1 %collective-permute-start.6 = (bf16[192,2048]{1,0:T(8,128)(2,1)S(1)}, bf16[192,2048]{1,0:T(8,128)(2,1)S(1)}, u32[]{:S(2)}, u32[]{:S(2)}) collective-permute-start(bf16[192,2048]{1,0:T(8,128)(2,1)S(1)} %get-tuple-element.51), channel_id=1, source_target_pairs={{0,4},{4,0},{8,12},{12,8},{16,20},{20,16},{24,28},{28,24},{1,5},{5... | collective-permute-start | bytes 2359304 | tf_op jit(solution)/shard_map/ppermute | solution.py:434
  191.1 77.2 %collective-permute-start.7 = (bf16[192,2048]{1,0:T(8,128)(2,1)S(1)}, bf16[192,2048]{1,0:T(8,128)(2,1)S(1)}, u32[]{:S(2)}, u32[]{:S(2)}) collective-permute-start(bf16[192,2048]{1,0:T(8,128)(2,1)S(1)} %get-tuple-element.50), channel_id=1, source_target_pairs={{0,8},{4,12},{8,0},{12,4},{16,24},{20,28},{24,16},{28,20},{1,9},{5... | collective-permute-start | bytes 2359304 | tf_op jit(solution)/shard_map/ppermute | solution.py:434
  218.5 65.0 %collective-permute-start.8 = (bf16[192,2048]{1,0:T(8,128)(2,1)S(1)}, bf16[192,2048]{1,0:T(8,128)(2,1)S(1)}, u32[]{:S(2)}, u32[]{:S(2)}) collective-permute-start(bf16[192,2048]{1,0:T(8,128)(2,1)S(1)} %get-tuple-element.49), channel_id=1, source_target_pairs={{0,12},{4,8},{8,4},{12,0},{16,28},{20,24},{24,20},{28,16},{1,13},{... | collective-permute-start | bytes 2359304 | tf_op jit(solution)/shard_map/ppermute | solution.py:434
  224.8 64.4 %collective-permute-start.16 = (bf16[384,2048]{1,0:T(8,128)(2,1)S(1)}, bf16[384,2048]{1,0:T(8,128)(2,1)S(1)}, u32[]{:S(2)}, u32[]{:S(2)}) collective-permute-start(bf16[384,2048]{1,0:T(8,128)(2,1)S(1)} %add_convert_fusion), channel_id=1, source_target_pairs={{0,16},{4,20},{8,24},{12,28},{16,0},{20,4},{24,8},{28,12},{1,17},{... | collective-permute-start | bytes 4718600 | tf_op jit(solution)/shard_map/ppermute | solution.py:373
  (11 other events, 43.1 us)
where the time goes:
time: 292 us
  waiting for transfers between devices  177 us (61%)
  matrix products  54.9 us (19%)
  starting transfers between devices  28.7 us (10%)
  Pallas kernels  22.3 us (8%)
  local copies, waits for them, and re-layouts  4.8 us (2%)
  other arithmetic  3.5 us (1%)
    ppermute x12, waiting for transfers between devices, swapped(): lax.ppermute(blocks[bits], 'sp', [(d, d ^ bits) for d in range(devices)])  175 us
    pallas_call x1, Pallas kernels, mixer(): pl.pallas_call(functools.partial(mixer_kernel, devices), grid=(pairs + ro...  22.3 us
    ppermute x3, starting transfers between devices, hop(): return lax.ppermute(array, 'sp', pairs)  13.4 us
    ppermute x12, starting transfers between devices, swapped(): lax.ppermute(blocks[bits], 'sp', [(d, d ^ bits) for d in range(devices)])  12.3 us
    dot_general x2, matrix products, experts(): jnp.dot(rows, expert_gate_weight[0], preferred_element_type=jnp.float32)  10.7 us
    dot_general x2, matrix products, experts(): up = jnp.dot(rows, expert_up_weight[0], preferred_element_type=jnp.float32)  9.26 us
    dot_general x2, matrix products, experts(): jnp.dot(hidden, expert_down_weight[0], preferred_element_type=jnp.float32)  7.79 us
    dot_general x3, matrix products, pick_rows(): lax.dot_general(chosen.astype(jnp.bfloat16), rows, (((0,), (0,)), ((), ()...  7.47 us
  transfers between devices with their start and end apart: 17, of which 12 were waited for; matrix products, arithmetic and copies ran while one was open for 15% of the time, Pallas kernels for 8%

commit v1 on v0

--- a/solution.py
+++ b/solution.py
@@ -45,7 +45,9 @@
     gate_ref,
     floor_ref,
     extra_ref,
+    share_ref,
     out_ref,
+    shares_ref,
     local_ref,
     decayed_ref,
     send_ref,
@@ -56,14 +58,44 @@
     upto_log_ref,
     send_sem,
     recv_sem,
+    share_send_sem,
+    share_recv_sem,
+    share_sem,
 ):
     rows = q_ref.shape[1]
     pairs = local_ref.shape[0]
     rounds = send_ref.shape[0]
-    heads = extra_ref.shape[1] // 3
+    heads = extra_ref.shape[1]
     step = pl.program_id(0)
     place = lax.axis_index("sp")
     first = iota((1, PAIR), 1) < HEAD_CHANNELS
+    copies = shares_ref.shape[0]
+    my_copy = lax.axis_index("dp")
+
+    def partner(source, step):
+        return source + step - 2 * step * ((source // step) % 2)
+
+    hand_overs = []
+    held = [my_copy]
+    stride = copies // 2
+    while stride:
+        hand_overs.append([(source, stride) for source in held])
+        held = held + [partner(source, stride) for source in held]
+        stride //= 2
+
+    def hand_over(stage, number):
+        source, stride = hand_overs[stage][number]
+        return pltpu.make_async_remote_copy(
+            src_ref=share_ref if number == 0 else shares_ref.at[source],
+            dst_ref=shares_ref.at[source],
+            send_sem=share_send_sem.at[stage, number],
+            recv_sem=share_recv_sem.at[stage, number],
+            device_id={"dp": partner(my_copy, stride)},
+            device_id_type=pl.DeviceIdType.MESH,
+        )
+
+    def keep_share():
+        return pltpu.make_async_copy(share_ref, shares_ref.at[my_copy], share_sem)
 
     def copy(number, pair):
         return pltpu.make_async_remote_copy(
@@ -100,17 +132,27 @@
                     device_id={"sp": lax.rem(other, devices)},
                     device_id_type=pl.DeviceIdType.MESH,
                 )
-        pl.semaphore_wait(barrier, 2 * rounds)
+        for group in hand_overs:
+            pl.semaphore_signal(
+                barrier,
+                inc=1,
+                device_id={"dp": partner(my_copy, group[0][1])},
+                device_id_type=pl.DeviceIdType.MESH,
+            )
+        pl.semaphore_wait(barrier, 2 * rounds + len(hand_overs))
+        keep_share().start()
+        for stage in range(len(hand_overs)):
+            hand_over(stage, 0).start()
 
     @pl.when(step < pairs)
     def _():
         pair = step
         blocks = rows // BLOCK
         spread = (
-            iota((3 * heads, PAIR), 0) % heads
-            == 2 * pair + iota((3 * heads, PAIR), 1) // HEAD_CHANNELS
+            iota((heads, PAIR), 0) == 2 * pair + iota((heads, PAIR), 1) // HEAD_CHANNELS
         ).astype(jnp.float32)
-        extra = dot_bf16(extra_ref[...], spread)
+        high, middle, low = (dot_bf16(third, spread) for third in three_parts(extra_ref[...]))
+        extra = high + (middle + low)
         same_head = (
             iota((PAIR, PAIR), 0) // HEAD_CHANNELS == iota((PAIR, PAIR), 1) // HEAD_CHANNELS
         )
@@ -215,8 +257,22 @@
         gate = gate / (1.0 + jnp.exp(-gate))
         out_ref[...] = (value * lax.rsqrt(mean + 1e-06) * gate).astype(jnp.bfloat16)
 
+    @pl.when(step == pairs + rounds - 2)
+    def _():
+        for stage in range(1, len(hand_overs)):
+            for number in range(len(hand_overs[stage - 1])):
+                hand_over(stage - 1, number).wait_recv()
+            for number in range(1, len(hand_overs[stage])):
+                hand_over(stage, number).start()
+
     @pl.when(step == pairs + rounds - 1)
     def _():
+        keep_share().wait()
+        for stage, group in enumerate(hand_overs):
+            for number in range(len(group)):
+                hand_over(stage, number).wait_send()
+                if stage == len(hand_overs) - 1:
+                    hand_over(stage, number).wait_recv()
         for number in range(rounds):
 
             @pl.when(place + 2**number < devices)
@@ -225,7 +281,7 @@
                     copy(number, pair).wait_send()
 
 
-def mixer(query, forget, value, gate, floor, extra, devices):
+def mixer(query, forget, value, gate, floor, extra, share, devices, copies):
     rows, width = query.shape[1:]
     pairs = width // PAIR
     rounds = (devices - 1).bit_length()
@@ -240,10 +296,17 @@
             early,
             late,
             pl.BlockSpec((1, PAIR), lambda s: (0, jnp.minimum(s, pairs - 1))),
-            pl.BlockSpec((rows, extra.shape[1] * 3), lambda s: (0, 0)),
+            pl.BlockSpec((rows, extra.shape[1]), lambda s: (0, 0)),
+            pl.BlockSpec(memory_space=pltpu.VMEM),
         ],
-        out_specs=pl.BlockSpec((rows, PAIR), lambda s: (0, jnp.maximum(s - rounds, 0))),
-        out_shape=jax.ShapeDtypeStruct((rows, width), jnp.bfloat16),
+        out_specs=[
+            pl.BlockSpec((rows, PAIR), lambda s: (0, jnp.maximum(s - rounds, 0))),
+            pl.BlockSpec(memory_space=pl.ANY),
+        ],
+        out_shape=[
+            jax.ShapeDtypeStruct((rows, width), jnp.bfloat16),
+            jax.ShapeDtypeStruct((copies,) + share.shape, share.dtype),
+        ],
         scratch_shapes=[
             pltpu.VMEM((pairs, rows, PAIR), jnp.float32),
             pltpu.VMEM((pairs, rows, PAIR), jnp.bfloat16),
@@ -255,6 +318,9 @@
             pltpu.VMEM((pairs, 8, PAIR), jnp.float32),
             pltpu.SemaphoreType.DMA((rounds, pairs)),
             pltpu.SemaphoreType.DMA((rounds, pairs)),
+            pltpu.SemaphoreType.DMA((copies.bit_length() - 1, copies // 2)),
+            pltpu.SemaphoreType.DMA((copies.bit_length() - 1, copies // 2)),
+            pltpu.SemaphoreType.DMA,
         ],
         compiler_params=pltpu.CompilerParams(collective_id=0, has_side_effects=True),
         cost_estimate=pl.CostEstimate(
@@ -266,7 +332,8 @@
         value,
         gate,
         floor.reshape(1, width),
-        jnp.concatenate(three_parts(extra), axis=1),
+        extra,
+        share,
     )
 
 
@@ -327,8 +394,6 @@
     my_group, my_local = place // GROUP, place % GROUP
 
     copies = lax.axis_size("dp")
-    my_copy = lax.axis_index("dp")
-
     picks = routes.reshape(tok_rows, 2)
     weights = routing_weight.reshape(tok_rows, 2)
     relative = (picks[:, :1] // GROUP - my_group + groups) % groups
@@ -357,7 +422,6 @@
             )
         )
 
-    own_plan = plan(own_local)
     leaves = positions_of(relative == jnp.arange(1, groups, dtype=jnp.int32)[None, :])
     place_in_group = iota((tok_rows, group_capacity), 1).astype(jnp.float32)
     crossing = jnp.concatenate(
@@ -375,41 +439,20 @@
     def part(array, number, size):
         return lax.slice_in_dim(array, number * size, (number + 1) * size, axis=0)
 
-    told = [
-        hop(part(noted, distance - 1, group_capacity), distance)
-        for distance in range(1, groups)
-    ]
-
     extra = lax.dynamic_slice_in_dim(extra_log_decay[0], place * tok_rows, tok_rows, 0)
-    mixer_out = mixer(
+    mixer_out, shares = mixer(
         query_weight,
         forget_preactivation,
         written_input,
         output_gate_logit,
         forget_floor,
         extra,
+        output_weight,
         devices,
-    )
-
-    shares = output_weight
-    step = copies // 2
-    order = [0]
-    while step:
-        other = lax.ppermute(shares, "dp", [(d, d ^ step) for d in range(copies)])
-        if step == copies // 2:
-            other, mixer_out = lax.optimization_barrier((other, mixer_out))
-        shares = jnp.concatenate([shares, other], axis=0)
-        order = order + [held ^ step for held in order]
-        step //= 2
-
-    share_width = mix_width // copies
-    mixer_out = jnp.concatenate(
-        [
-            lax.dynamic_slice_in_dim(mixer_out, (my_copy ^ held) * share_width, share_width, 1)
-            for held in order
-        ],
-        axis=1,
-    )
+        copies,
+    )
+
+    shares = shares.reshape(mix_width, model_width)
     projected = jnp.dot(mixer_out, shares, preferred_element_type=jnp.float32)
     updated = (residual.reshape(tok_rows, model_width).astype(jnp.float32) + projected).astype(
         jnp.bfloat16
@@ -424,7 +467,7 @@
     def experts(rows):
         gate = jnp.dot(rows, expert_gate_weight[0], preferred_element_type=jnp.float32)
         up = jnp.dot(rows, expert_up_weight[0], preferred_element_type=jnp.float32)
-        hidden = (jax.nn.silu(gate) * up).astype(jnp.bfloat16)
+        hidden = lax.optimization_barrier((jax.nn.silu(gate) * up).astype(jnp.bfloat16))
         return jnp.dot(
             hidden, expert_down_weight[0], preferred_element_type=jnp.float32
         ).astype(jnp.bfloat16)
@@ -444,9 +487,16 @@
         hop(part(leaving, distance - 1, group_capacity), distance)
         for distance in range(1, groups)
     ]
-    own_rows = pick_rows(own_plan, normed)
-    late = (weights, own_plan, *told, own_rows)
-    weights, own_plan, *told, own_rows = lax.optimization_barrier(late)
+    own_local, late_normed = lax.optimization_barrier((own_local, normed))
+    own_plan = plan(own_local)
+    own_rows = pick_rows(own_plan, late_normed)
+    late = (weights, own_plan, noted, own_rows)
+    weights, own_plan, noted, own_rows = lax.optimization_barrier(late)
+    told = [
+        hop(part(noted, distance - 1, group_capacity), distance)
+        for distance in range(1, groups)
+    ]
+
     own = swapped(blocks_of(own_rows))
     locals_told = [jnp.round(t[:, :2]).astype(jnp.int32) - 1 for t in told]
     plans = [plan(local) for local in locals_told]
@@ -458,8 +508,13 @@
     own_made = experts(jnp.concatenate(own, axis=0))
     back = []
     for number, blocks in enumerate(given, 1):
-        made = experts(jnp.concatenate(blocks, axis=0))
-        made = swapped(blocks_of(made))
+        middle = GROUP // 2
+        near = experts(jnp.concatenate(blocks[:middle], axis=0))
+        across_z = experts(jnp.concatenate(blocks[middle:], axis=0))
+        made = swapped(
+            [part(near, bits, capacity) for bits in range(middle)]
+            + [part(across_z, bits, capacity) for bits in range(GROUP - middle)]
+        )
         total = weigh_rows(tables[number], jnp.concatenate(made, axis=0)).astype(jnp.bfloat16)
         back.append(hop(total, groups - number))
     own_made = jnp.concatenate(swapped(blocks_of(own_made)), axis=0)

time: 292 us -> 294 us (level)
  Pallas kernels: 22.3 us -> 36 us
  starting transfers between devices: 28.7 us -> 22 us
  waiting for transfers between devices: 177 us -> 173 us
    pallas_call x1, Pallas kernels: 22.3 us -> 36 us  [mixer(): pl.pallas_call(functools.partial(mixer_kernel, devices), grid=(pairs + ro...]
    ppermute x12, waiting for transfers between devices: 175 us -> 168 us  [swapped(): lax.ppermute(blocks[bits], 'sp', [(d, d ^ bits) for d in range(devices)])]
    ppermute x3, starting transfers between devices: 13.4 us -> 7.67 us  [hop(): return lax.ppermute(array, 'sp', pairs)]
    ppermute x2 -> x0, starting transfers between devices: 3.04 us -> none  [per_device(): other = lax.ppermute(shares, 'dp', [(d, d ^ step) for d in range(copies)])]
    dot_general x2 -> x3, matrix products: 7.79 us -> 7.27 us  [experts(): jnp.dot(hidden, expert_down_weight[0], preferred_element_type=jnp.float32)]
    dot_general x2 -> x3, matrix products: 10.7 us -> 10.2 us  [experts(): jnp.dot(rows, expert_gate_weight[0], preferred_element_type=jnp.float32)]
    dot_general x2 -> x3, matrix products: 9.26 us -> 9.71 us  [experts(): up = jnp.dot(rows, expert_up_weight[0], preferred_element_type=jnp.float32)]
  transfers between devices with their start and end apart: 17 -> 15, of which waited for: 12 -> 11; matrix products, arithmetic and copies ran while one was open for 15% -> 14% of each run, Pallas kernels for 8% -> 0%
where the time goes in v1:
time: 294 us
  waiting for transfers between devices  173 us (59%)
  matrix products  53.8 us (18%)
  Pallas kernels  36 us (12%)
  starting transfers between devices  22 us (7%)
  local copies, waits for them, and re-layouts  5.95 us (2%)
    ppermute x12, waiting for transfers between devices, swapped(): lax.ppermute(blocks[bits], 'sp', [(d, d ^ bits) for d in range(devices)])  168 us
    pallas_call x1, Pallas kernels, mixer(): pl.pallas_call(functools.partial(mixer_kernel, devices), grid=(pairs + ro...  36 us
    ppermute x12, starting transfers between devices, swapped(): lax.ppermute(blocks[bits], 'sp', [(d, d ^ bits) for d in range(devices)])  14.3 us
    dot_general x3, matrix products, experts(): jnp.dot(rows, expert_gate_weight[0], preferred_element_type=jnp.float32)  10.2 us
    dot_general x3, matrix products, experts(): up = jnp.dot(rows, expert_up_weight[0], preferred_element_type=jnp.float32)  9.71 us
    dot_general x3, matrix products, pick_rows(): lax.dot_general(chosen.astype(jnp.bfloat16), rows, (((0,), (0,)), ((), ()...  8.84 us
    ppermute x3, starting transfers between devices, hop(): return lax.ppermute(array, 'sp', pairs)  7.67 us
    dot_general x3, matrix products, experts(): jnp.dot(hidden, expert_down_weight[0], preferred_element_type=jnp.float32)  7.27 us
  transfers between devices with their start and end apart: 15, of which 11 were waited for; matrix products, arithmetic and copies ran while one was open for 14% of the time, Pallas kernels for 0%

profile of v1, /device:TPU:0, one launch (start us, length us, event | category | flops | bytes accessed | tf_op | source)
XLA Modules:
  0.0 293.9 jit_solution(1488448406153443277)
XLA Ops:
  1.7 36.0 %shard_map.136 = (bf16[384,1024]{1,0:T(8,128)(2,1)}, bf16[4,256,2048]{2,1,0:T(8,128)(2,1)}) custom-call(bf16[1,384,1024]{2,1,0:T(8,128)(2,1)} %q_ref.1, bf16[1,384,1024]{2,1,0:T(8,128)(2,1)} %f_ref.1, bf16[1,384,1024]{2,1,0:T(8,128)(2,1)} %v_ref.1, bf16[1,384,1024]{2,1,0:T(8,128)(2,1)} %gate_ref.1, f32[1,1024]{1,0:T(1,128)} %bitcast.72, f32[384,16]{1,0:T(8,128)} %bitcast.68, ...), custom_call_target="tpu_custom_call" | custom-call | flops 2516582400 | bytes 3932160 | tf_op jit(solution)/shard_map/pallas_call | solution.py:290
  37.7 4.9 %fusion.21 = (f32[384]{0:T(512)S(1)}, bf16[384,2048]{1,0:T(8,128)(2,1)S(1)}) fusion(bf16[384,1024]{1,0:T(8,128)(2,1)} %get-tuple-element.17, bf16[1024,2048]{1,0:T(8,128)(2,1)} %bitcast.73, bf16[1,384,2048]{2,1,0:T(8,128)(2,1)} %param.20), kind=kOutput, calls=%fused_computation.24 | convolution fusion | flops 1615330944 | bytes 8128000 | tf_op jit(solution)/shard_map/dot_general | solution.py:456
  45.4 3.4 %convolution_convert_fusion.1 = bf16[768,2048]{1,0:T(8,128)(2,1)S(1)} fusion(bf16[384,768]{1,0:T(8,128)(2,1)S(1)} %fusion.37, bf16[384,2048]{1,0:T(8,128)(2,1)} %fusion.23), kind=kOutput, calls=%fused_computation.23 | convolution fusion | flops 1209532416 | bytes 5308416 | tf_op jit(solution)/shard_map/dot_general | solution.py:356
  49.2 2.2 convolution_convert_fusion.2
  51.5 2.8 collective-permute-start.7
  57.2 2.3 collective-permute-start.2
  61.3 14.6 %collective-permute-done = bf16[192,2048]{1,0:T(8,128)(2,1)} collective-permute-done((bf16[192,2048]{1,0:T(8,128)(2,1)}, bf16[192,2048]{1,0:T(8,128)(2,1)}, u32[]{:S(2)}, u32[]{:S(2)}) %collective-permute-start) | collective-permute-done | bytes 786464 | tf_op jit(solution)/shard_map/ppermute | solution.py:477
  75.8 30.5 %collective-permute-done.1 = bf16[192,2048]{1,0:T(8,128)(2,1)} collective-permute-done((bf16[192,2048]{1,0:T(8,128)(2,1)}, bf16[192,2048]{1,0:T(8,128)(2,1)}, u32[]{:S(2)}, u32[]{:S(2)}) %collective-permute-start.1) | collective-permute-done | bytes 786464 | tf_op jit(solution)/shard_map/ppermute | solution.py:477
  106.3 19.0 %collective-permute-done.2 = bf16[192,2048]{1,0:T(8,128)(2,1)} collective-permute-done((bf16[192,2048]{1,0:T(8,128)(2,1)}, bf16[192,2048]{1,0:T(8,128)(2,1)}, u32[]{:S(2)}, u32[]{:S(2)}) %collective-permute-start.2) | collective-permute-done | bytes 786464 | tf_op jit(solution)/shard_map/ppermute | solution.py:477
  125.3 6.6 %fusion.16 = f32[768,1024]{1,0:T(8,128)S(1)} fusion(bf16[1,2048,1024]{2,1,0:T(8,128)(2,1)} %param.23, bf16[192,2048]{1,0:T(8,128)(2,1)} %collective-permute-done.2, bf16[192,2048]{1,0:T(8,128)(2,1)} %collective-permute-done.1, bf16[192,2048]{1,0:T(8,128)(2,1)} %collective-permute-done, bf16[192,2048]{1,0:T(8,128)(2,1)} %get-tuple-element.49), kind=kOutput, calls=%fused_computation.19 | convolution fusion | flops 3233808384 | bytes 10485760 | tf_op jit(solution)/shard_map/dot_general | solution.py:468
  131.9 3.2 %convolution_convert_fusion = bf16[768,2048]{1,0:T(8,128)(2,1)S(1)} fusion(bf16[384,768]{1,0:T(8,128)(2,1)S(1)} %fusion.38, bf16[384,2048]{1,0:T(8,128)(2,1)} %collective-permute-done.7), kind=kOutput, calls=%fused_computation.22 | convolution fusion | flops 1209532416 | bytes 5308416 | tf_op jit(solution)/shard_map/dot_general | solution.py:356
  137.5 5.7 %multiply_convert_fusion = bf16[768,1024]{1,0:T(8,128)(2,1)S(1)} fusion(f32[768,1024]{1,0:T(8,128)S(1)} %fusion.16, bf16[1,2048,1024]{2,1,0:T(8,128)(2,1)S(1)} %copy-done.8, bf16[192,2048]{1,0:T(8,128)(2,1)} %collective-permute-done.2, bf16[192,2048]{1,0:T(8,128)(2,1)} %collective-permute-done.1, bf16[192,2048]{1,0:T(8,128)(2,1)} %collective-permute-done, ...), kind=kOutput, calls=%fused_computation.34 | convolution fusion | flops 3238526976 | bytes 12058624 | tf_op jit(solution)/shard_map/dot_general | solution.py:469
  144.9 6.4 %collective-permute-done.8 = bf16[192,2048]{1,0:T(8,128)(2,1)S(1)} collective-permute-done((bf16[192,2048]{1,0:T(8,128)(2,1)S(1)}, bf16[192,2048]{1,0:T(8,128)(2,1)S(1)}, u32[]{:S(2)}, u32[]{:S(2)}) %collective-permute-start.8) | collective-permute-done | bytes 786464 | tf_op jit(solution)/shard_map/ppermute | solution.py:477
  157.9 5.9 %collective-permute-done.10 = bf16[192,2048]{1,0:T(8,128)(2,1)S(1)} collective-permute-done((bf16[192,2048]{1,0:T(8,128)(2,1)S(1)}, bf16[192,2048]{1,0:T(8,128)(2,1)S(1)}, u32[]{:S(2)}, u32[]{:S(2)}) %collective-permute-start.10) | collective-permute-done | bytes 786464 | tf_op jit(solution)/shard_map/ppermute | solution.py:477
  163.9 13.8 %collective-permute-done.11 = bf16[192,2048]{1,0:T(8,128)(2,1)S(1)} collective-permute-done((bf16[192,2048]{1,0:T(8,128)(2,1)S(1)}, bf16[192,2048]{1,0:T(8,128)(2,1)S(1)}, u32[]{:S(2)}, u32[]{:S(2)}) %collective-permute-start.11) | collective-permute-done | bytes 786464 | tf_op jit(solution)/shard_map/ppermute | solution.py:477
  185.6 3.6 %fusion.18 = bf16[768,2048]{1,0:T(8,128)(2,1)S(1)} fusion(bf16[768,1024]{1,0:T(8,128)(2,1)S(1)} %multiply_convert_fusion, bf16[1,1024,2048]{2,1,0:T(8,128)(2,1)S(1)} %copy-done.9), kind=kOutput, calls=%fused_computation.21 | convolution fusion | flops 3222798336 | bytes 8912896 | tf_op jit(solution)/shard_map/dot_general | solution.py:471
  192.8 3.2 %collective-permute-start.5 = (bf16[192,2048]{1,0:T(8,128)(2,1)S(1)}, bf16[192,2048]{1,0:T(8,128)(2,1)S(1)}, u32[]{:S(2)}, u32[]{:S(2)}) collective-permute-start(bf16[192,2048]{1,0:T(8,128)(2,1)S(1)} %get-tuple-element.46), channel_id=1, source_target_pairs={{0,12},{4,8},{8,4},{12,0},{16,28},{20,24},{24,20},{28,16},{1,13},{... | collective-permute-start | bytes 2359304 | tf_op jit(solution)/shard_map/ppermute | solution.py:477
  195.9 8.1 %collective-permute-done.12 = bf16[192,2048]{1,0:T(8,128)(2,1)S(1)} collective-permute-done((bf16[192,2048]{1,0:T(8,128)(2,1)S(1)}, bf16[192,2048]{1,0:T(8,128)(2,1)S(1)}, u32[]{:S(2)}, u32[]{:S(2)}) %collective-permute-start.12) | collective-permute-done | bytes 786464 | tf_op jit(solution)/shard_map/ppermute | solution.py:477
  204.0 16.9 %collective-permute-done.13 = bf16[192,2048]{1,0:T(8,128)(2,1)S(1)} collective-permute-done((bf16[192,2048]{1,0:T(8,128)(2,1)S(1)}, bf16[192,2048]{1,0:T(8,128)(2,1)S(1)}, u32[]{:S(2)}, u32[]{:S(2)}) %collective-permute-start.13) | collective-permute-done | bytes 786464 | tf_op jit(solution)/shard_map/ppermute | solution.py:477
  224.2 4.7 %collective-permute-start.14 = (bf16[384,2048]{1,0:T(8,128)(2,1)S(1)}, bf16[384,2048]{1,0:T(8,128)(2,1)S(1)}, u32[]{:S(2)}, u32[]{:S(2)}) collective-permute-start(bf16[384,2048]{1,0:T(8,128)(2,1)S(1)} %add_convert_fusion), channel_id=1, source_target_pairs={{0,16},{4,20},{8,24},{12,28},{16,0},{20,4},{24,8},{28,12},{1,17},{... | collective-permute-start | bytes 4718600 | tf_op jit(solution)/shard_map/ppermute | solution.py:437
  229.9 38.8 %collective-permute-done.4 = bf16[192,2048]{1,0:T(8,128)(2,1)S(1)} collective-permute-done((bf16[192,2048]{1,0:T(8,128)(2,1)S(1)}, bf16[192,2048]{1,0:T(8,128)(2,1)S(1)}, u32[]{:S(2)}, u32[]{:S(2)}) %collective-permute-start.4) | collective-permute-done | bytes 786464 | tf_op jit(solution)/shard_map/ppermute | solution.py:477
  268.7 14.5 %collective-permute-done.5 = bf16[192,2048]{1,0:T(8,128)(2,1)S(1)} collective-permute-done((bf16[192,2048]{1,0:T(8,128)(2,1)S(1)}, bf16[192,2048]{1,0:T(8,128)(2,1)S(1)}, u32[]{:S(2)}, u32[]{:S(2)}) %collective-permute-start.5) | collective-permute-done | bytes 786464 | tf_op jit(solution)/shard_map/ppermute | solution.py:477
  286.5 5.0 %collective-permute-done.14 = bf16[384,2048]{1,0:T(8,128)(2,1)S(1)} collective-permute-done((bf16[384,2048]{1,0:T(8,128)(2,1)S(1)}, bf16[384,2048]{1,0:T(8,128)(2,1)S(1)}, u32[]{:S(2)}, u32[]{:S(2)}) %collective-permute-start.14) | collective-permute-done | bytes 1572896 | tf_op jit(solution)/shard_map/ppermute | solution.py:437
  291.4 2.5 fusion.32
  (81 shorter events, 39.1 us)
Async XLA Ops:
  37.7 5.0 %copy-start.5 = (s32[1,384,2]{1,2,0:T(2,128)S(1)}, s32[1,384,2]{1,2,0:T(2,128)}, u32[]{:S(2)}) copy-start(s32[1,384,2]{1,2,0:T(2,128)} %param.26) | copy-start | bytes 9220
  37.7 5.0 %copy-start.4 = (f32[2048]{0:T(1024)S(1)}, f32[2048]{0:T(1024)}, u32[]{:S(2)}) copy-start(f32[2048]{0:T(1024)} %param.22) | copy-start | bytes 24580
  45.3 3.4 %copy-start.6 = (f32[1,384,2]{1,2,0:T(2,128)S(1)}, f32[1,384,2]{1,2,0:T(2,128)}, u32[]{:S(2)}) copy-start(f32[1,384,2]{1,2,0:T(2,128)} %param.27) | copy-start | bytes 9220
  45.3 3.9 %copy-start.2 = (bf16[384,2048]{1,0:T(8,128)(2,1)S(1)}, bf16[384,2048]{1,0:T(8,128)(2,1)}, u32[]{:S(2)}) copy-start(bf16[384,2048]{1,0:T(8,128)(2,1)} %fusion.23) | copy-start | bytes 4718596
  49.1 10.4 %collective-permute-start.6 = (f32[384,4]{0,1:T(4,128)S(1)}, f32[384,4]{0,1:T(4,128)S(1)}, u32[]{:S(2)}, u32[]{:S(2)}) collective-permute-start(f32[384,4]{0,1:T(4,128)S(1)} %fusion.46), channel_id=1, source_target_pairs={{0,16},{4,20},{8,24},{12,28},{16,0},{20,4},{24,8},{28,12},{1,17},{... | collective-permute-start | bytes 18440 | tf_op jit(solution)/shard_map/ppermute | solution.py:437
  51.5 80.4 %collective-permute-start.7 = (bf16[384,2048]{1,0:T(8,128)(2,1)}, bf16[384,2048]{1,0:T(8,128)(2,1)}, u32[]{:S(2)}, u32[]{:S(2)}) collective-permute-start(bf16[384,2048]{1,0:T(8,128)(2,1)} %convolution_convert_fusion.2), channel_id=1, source_target_pairs={{0,16},{4,20},{8,24},{12,28},{16,0},{20,4},{24,8},{28,12},{1,17},{... | collective-permute-start | bytes 4718600 | tf_op jit(solution)/shard_map/ppermute | solution.py:437
  56.0 19.8 %collective-permute-start = (bf16[192,2048]{1,0:T(8,128)(2,1)}, bf16[192,2048]{1,0:T(8,128)(2,1)}, u32[]{:S(2)}, u32[]{:S(2)}) collective-permute-start(bf16[192,2048]{1,0:T(8,128)(2,1)} %get-tuple-element.52), channel_id=1, source_target_pairs={{0,4},{4,0},{8,12},{12,8},{16,20},{20,16},{24,28},{28,24},{1,5},{5... | collective-permute-start | bytes 2359304 | tf_op jit(solution)/shard_map/ppermute | solution.py:477
  56.6 49.7 %collective-permute-start.1 = (bf16[192,2048]{1,0:T(8,128)(2,1)}, bf16[192,2048]{1,0:T(8,128)(2,1)}, u32[]{:S(2)}, u32[]{:S(2)}) collective-permute-start(bf16[192,2048]{1,0:T(8,128)(2,1)} %get-tuple-element.51), channel_id=1, source_target_pairs={{0,8},{4,12},{8,0},{12,4},{16,24},{20,28},{24,16},{28,20},{1,9},{5... | collective-permute-start | bytes 2359304 | tf_op jit(solution)/shard_map/ppermute | solution.py:477
  57.2 68.1 %collective-permute-start.2 = (bf16[192,2048]{1,0:T(8,128)(2,1)}, bf16[192,2048]{1,0:T(8,128)(2,1)}, u32[]{:S(2)}, u32[]{:S(2)}) collective-permute-start(bf16[192,2048]{1,0:T(8,128)(2,1)} %get-tuple-element.50), channel_id=1, source_target_pairs={{0,12},{4,8},{8,4},{12,0},{16,28},{20,24},{24,20},{28,16},{1,13},{... | collective-permute-start | bytes 2359304 | tf_op jit(solution)/shard_map/ppermute | solution.py:477
  135.1 1.1 copy-start.3
  135.1 2.4 copy-start.8
  135.5 15.7 %copy-start.7 = (bf16[1,2048,1024]{2,1,0:T(8,128)(2,1)S(1)}, bf16[1,2048,1024]{2,1,0:T(8,128)(2,1)}, u32[]{:S(2)}) copy-start(bf16[1,2048,1024]{2,1,0:T(8,128)(2,1)} %param.23) | copy-start | bytes 12582916
  135.6 15.7 %collective-permute-start.8 = (bf16[192,2048]{1,0:T(8,128)(2,1)S(1)}, bf16[192,2048]{1,0:T(8,128)(2,1)S(1)}, u32[]{:S(2)}, u32[]{:S(2)}) collective-permute-start(bf16[192,2048]{1,0:T(8,128)(2,1)S(1)} %get-tuple-element.44), channel_id=1, source_target_pairs={{0,4},{4,0},{8,12},{12,8},{16,20},{20,16},{24,28},{28,24},{1,5},{5... | collective-permute-start | bytes 2359304 | tf_op jit(solution)/shard_map/ppermute | solution.py:477
  143.3 20.5 %collective-permute-start.10 = (bf16[192,2048]{1,0:T(8,128)(2,1)S(1)}, bf16[192,2048]{1,0:T(8,128)(2,1)S(1)}, u32[]{:S(2)}, u32[]{:S(2)}) collective-permute-start(bf16[192,2048]{1,0:T(8,128)(2,1)S(1)} %get-tuple-element.43), channel_id=1, source_target_pairs={{0,8},{4,12},{8,0},{12,4},{16,24},{20,28},{24,16},{28,20},{1,9},{5... | collective-permute-start | bytes 2359304 | tf_op jit(solution)/shard_map/ppermute | solution.py:477
  143.4 34.2 %collective-permute-start.11 = (bf16[192,2048]{1,0:T(8,128)(2,1)S(1)}, bf16[192,2048]{1,0:T(8,128)(2,1)S(1)}, u32[]{:S(2)}, u32[]{:S(2)}) collective-permute-start(bf16[192,2048]{1,0:T(8,128)(2,1)S(1)} %get-tuple-element.42), channel_id=1, source_target_pairs={{0,12},{4,8},{8,4},{12,0},{16,28},{20,24},{24,20},{28,16},{1,13},{... | collective-permute-start | bytes 2359304 | tf_op jit(solution)/shard_map/ppermute | solution.py:477
  153.1 2.2 copy-start.9
  157.3 35.5 %collective-permute-start.9 = (bf16[192,2048]{1,0:T(8,128)(2,1)S(1)}, bf16[192,2048]{1,0:T(8,128)(2,1)S(1)}, u32[]{:S(2)}, u32[]{:S(2)}) collective-permute-start(bf16[192,2048]{1,0:T(8,128)(2,1)S(1)} %get-tuple-element.54), channel_id=1, source_target_pairs={{0,4},{4,0},{8,12},{12,8},{16,20},{20,16},{24,28},{28,24},{1,5},{5... | collective-permute-start | bytes 2359304 | tf_op jit(solution)/shard_map/ppermute | solution.py:477
  183.5 20.5 %collective-permute-start.12 = (bf16[192,2048]{1,0:T(8,128)(2,1)S(1)}, bf16[192,2048]{1,0:T(8,128)(2,1)S(1)}, u32[]{:S(2)}, u32[]{:S(2)}) collective-permute-start(bf16[192,2048]{1,0:T(8,128)(2,1)S(1)} %get-tuple-element.55), channel_id=1, source_target_pairs={{0,8},{4,12},{8,0},{12,4},{16,24},{20,28},{24,16},{28,20},{1,9},{5... | collective-permute-start | bytes 2359304 | tf_op jit(solution)/shard_map/ppermute | solution.py:477
  185.3 35.6 %collective-permute-start.13 = (bf16[192,2048]{1,0:T(8,128)(2,1)S(1)}, bf16[192,2048]{1,0:T(8,128)(2,1)S(1)}, u32[]{:S(2)}, u32[]{:S(2)}) collective-permute-start(bf16[192,2048]{1,0:T(8,128)(2,1)S(1)} %get-tuple-element.56), channel_id=1, source_target_pairs={{0,12},{4,8},{8,4},{12,0},{16,28},{20,24},{24,20},{28,16},{1,13},{... | collective-permute-start | bytes 2359304 | tf_op jit(solution)/shard_map/ppermute | solution.py:477
  189.5 40.4 %collective-permute-start.3 = (bf16[192,2048]{1,0:T(8,128)(2,1)S(1)}, bf16[192,2048]{1,0:T(8,128)(2,1)S(1)}, u32[]{:S(2)}, u32[]{:S(2)}) collective-permute-start(bf16[192,2048]{1,0:T(8,128)(2,1)S(1)} %get-tuple-element.48), channel_id=1, source_target_pairs={{0,4},{4,0},{8,12},{12,8},{16,20},{20,16},{24,28},{28,24},{1,5},{5... | collective-permute-start | bytes 2359304 | tf_op jit(solution)/shard_map/ppermute | solution.py:477
  191.0 77.7 %collective-permute-start.4 = (bf16[192,2048]{1,0:T(8,128)(2,1)S(1)}, bf16[192,2048]{1,0:T(8,128)(2,1)S(1)}, u32[]{:S(2)}, u32[]{:S(2)}) collective-permute-start(bf16[192,2048]{1,0:T(8,128)(2,1)S(1)} %get-tuple-element.47), channel_id=1, source_target_pairs={{0,8},{4,12},{8,0},{12,4},{16,24},{20,28},{24,16},{28,20},{1,9},{5... | collective-permute-start | bytes 2359304 | tf_op jit(solution)/shard_map/ppermute | solution.py:477
  192.8 90.5 %collective-permute-start.5 = (bf16[192,2048]{1,0:T(8,128)(2,1)S(1)}, bf16[192,2048]{1,0:T(8,128)(2,1)S(1)}, u32[]{:S(2)}, u32[]{:S(2)}) collective-permute-start(bf16[192,2048]{1,0:T(8,128)(2,1)S(1)} %get-tuple-element.46), channel_id=1, source_target_pairs={{0,12},{4,8},{8,4},{12,0},{16,28},{20,24},{24,20},{28,16},{1,13},{... | collective-permute-start | bytes 2359304 | tf_op jit(solution)/shard_map/ppermute | solution.py:477
  224.2 67.3 %collective-permute-start.14 = (bf16[384,2048]{1,0:T(8,128)(2,1)S(1)}, bf16[384,2048]{1,0:T(8,128)(2,1)S(1)}, u32[]{:S(2)}, u32[]{:S(2)}) collective-permute-start(bf16[384,2048]{1,0:T(8,128)(2,1)S(1)} %add_convert_fusion), channel_id=1, source_target_pairs={{0,16},{4,20},{8,24},{12,28},{16,0},{20,4},{24,8},{28,12},{1,17},{... | collective-permute-start | bytes 4718600 | tf_op jit(solution)/shard_map/ppermute | solution.py:437
  284.9 9.1 %copy-start.1 = (f32[1,3072,16]{1,2,0:T(8,128)S(1)}, f32[1,3072,16]{1,2,0:T(8,128)}, u32[]{:S(2)}) copy-start(f32[1,3072,16]{1,2,0:T(8,128)} %param.19) | copy-start | bytes 589828
  (1 other events, 0.9 us)
